TPU v7x, 32 devices: a whole 2x2x4 slice. The times are simulated.
32 devices in a mesh: sp: 8 (over z, y), tp: 4 (over x, core).
Axes of the slice: x: 2, y: 2, z: 4, core: 2. Of those that a mesh axis runs over, the one named last changes fastest.
Arguments:
- queries: bfloat16 [1024, 1024], P('sp', 'tp'), may hold values from -600 to 600, as said below
- keys: bfloat16 [1024, 256], P('sp', 'tp'), may hold values from -6 to 6
- values: bfloat16 [1024, 256], P('sp', 'tp'), may hold values from -18 to 18
- forget_prefix_log: float32 [1024, 16], P('sp', 'tp'), as said below
- residual: bfloat16 [1024, 2048], P(('sp', 'tp')), may hold values from -6 to 6
- out_weight: bfloat16 [1024, 2048], replicated, may hold values from -0.1875 to 0.1875
- norm_gain: float32 [2048], replicated, may hold values from 0.1 to 1.9
- routes: int32 [1024, 2], P(('sp', 'tp')), may hold values from 0 to 7, all different within a row; in each aligned block of 32 rows (0 to 31, 32 to 63, ...) at most 16 rows name the same one
- route_weight: float32 [1024, 2], P(('sp', 'tp')), may hold values from 0.1 to 1
- w_gate: bfloat16 [8, 2048, 1024], P('sp', None, 'tp'), may hold values from -0.125 to 0.125
- w_up: bfloat16 [8, 2048, 1024], P('sp', None, 'tp'), may hold values from -0.125 to 0.125
- w_down: bfloat16 [8, 1024, 2048], P('sp', 'tp'), may hold values from -0.1875 to 0.1875
Outputs:
- layer_out: bfloat16 [1024, 2048], P(('sp', 'tp'))
Inputs may be any that keep to these rules, and one draw needn't show every extreme that they name: `queries`: queries are of order one except for a few positions. `forget_prefix_log`: never rising along positions. `routes`: within the rows of one device (32 positions in order), no expert is named by more than 16 rows, a bound that some block reaches; the experts of one row differ.
All inputs are finite; a program needn't handle non-finite values.
Results may differ from a plain program's by a relative error of at most 0.013.
Values may be sent and summed in bfloat16 or wider, within the bound.
A program may use at most 64 MiB of HBM per device.

v0:
```python
import math

import jax
import jax.numpy as jnp
from jax import lax
from jax.sharding import PartitionSpec as P

HEAD_DIM = 64


def shards(
    queries,
    keys,
    values,
    forget_prefix_log,
    residual,
    out_weight,
    norm_gain,
    routes,
    route_weight,
    w_gate,
    w_up,
    w_down,
):
    tok_dev = queries.shape[0]
    kv_local = keys.shape[1] // HEAD_DIM
    heads_local = forget_prefix_log.shape[1]
    group_size = heads_local // kv_local
    score_scale = HEAD_DIM ** (-0.5)
    offset = lax.axis_index("sp") * tok_dev
    query_pos = offset + jnp.arange(tok_dev, dtype=jnp.int32)
    last_query = offset + tok_dev - 1
    query_local = queries.reshape(tok_dev, kv_local, group_size, HEAD_DIM)
    shard_forget_factor = forget_prefix_log.reshape(tok_dev, kv_local, group_size).transpose(
        1, 2, 0
    )
    gates_all = lax.all_gather(forget_prefix_log, "sp", axis=0, tiled=True)

    def absorb_span(running_total, key_span, value_span, key_first):
        row_peak, row_total, weighted = running_total
        span = key_span.shape[0]
        key_heads = key_span.reshape(span, kv_local, HEAD_DIM)
        value_heads = value_span.reshape(span, kv_local, HEAD_DIM)
        gate_keys = lax.dynamic_slice_in_dim(gates_all, key_first, span, 0).reshape(
            span, kv_local, group_size
        )
        scores = (
            jnp.einsum("tkgd,nkd->kgtn", query_local, key_heads, preferred_element_type=jnp.float32)
            * score_scale
        )
        scores = (
            scores + shard_forget_factor[..., None] - gate_keys.transpose(1, 2, 0)[:, :, None, :]
        )
        causal = query_pos[:, None] >= (key_first + jnp.arange(span, dtype=jnp.int32))[None, :]
        scores = jnp.where(causal, scores, -1e30)
        new_peak = jnp.maximum(row_peak, jnp.max(scores, axis=-1))
        weights = jnp.where(causal, jnp.exp(scores - new_peak[..., None]), 0.0)
        shrink = jnp.exp(row_peak - new_peak)
        row_total = row_total * shrink + jnp.sum(weights, axis=-1)
        product = jnp.einsum(
            "kgtn,nkd->tkgd",
            weights.astype(jnp.bfloat16),
            value_heads,
            preferred_element_type=jnp.float32,
        )
        weighted = weighted * shrink.transpose(2, 0, 1)[..., None] + product
        return (new_peak, row_total, weighted)

    initial = (
        jnp.full((kv_local, group_size, tok_dev), -1e30, jnp.float32),
        jnp.zeros((kv_local, group_size, tok_dev), jnp.float32),
        jnp.zeros((tok_dev, kv_local, group_size, HEAD_DIM), jnp.float32),
    )
    key_piece = lax.all_gather(keys, "sp", axis=0, tiled=True)
    value_piece = lax.all_gather(values, "sp", axis=0, tiled=True)
    row_count = key_piece.shape[0]
    span = row_count if row_count <= 1024 else math.gcd(row_count, 1024)

    def one_span(span_index, inner_state):
        begin = span_index * span
        key_span = lax.dynamic_slice_in_dim(key_piece, begin, span, 0)
        value_span = lax.dynamic_slice_in_dim(value_piece, begin, span, 0)
        return lax.cond(
            begin <= last_query,
            lambda state: absorb_span(state, key_span, value_span, begin),
            lambda state: state,
            inner_state,
        )

    row_peak, row_total, weighted = lax.fori_loop(0, row_count // span, one_span, initial)
    attended = (weighted / row_total.transpose(2, 0, 1)[..., None]).astype(jnp.bfloat16)
    attended = attended.reshape(tok_dev, heads_local * HEAD_DIM)
    tensor_parallel_count = lax.axis_size("tp")
    tok_row = tok_dev // tensor_parallel_count
    swapped = lax.all_to_all(attended, "tp", split_axis=0, concat_axis=1, tiled=True)
    projected = jnp.dot(swapped, out_weight, preferred_element_type=jnp.float32)
    stream = residual.astype(jnp.float32) + projected
    mean_square = jnp.mean(stream * stream, axis=-1, keepdims=True)
    normed = (stream * lax.rsqrt(mean_square + 1e-06) * norm_gain).astype(jnp.bfloat16)
    model_width = normed.shape[1]
    expert_count = lax.axis_size("sp")
    top_count = routes.shape[1]
    capacity = max(2, 2 * tok_row * top_count // expert_count)
    flat_expert = routes.reshape(-1)
    onehot = (flat_expert[:, None] == jnp.arange(expert_count, dtype=jnp.int32)[None, :]).astype(
        jnp.int32
    )
    slot_rank = jnp.sum((jnp.cumsum(onehot, axis=0) - onehot) * onehot, axis=1)
    slot_index = flat_expert * capacity + slot_rank
    source_rows = normed[jnp.arange(flat_expert.shape[0], dtype=jnp.int32) // top_count]
    outgoing = (
        jnp.zeros((expert_count * capacity, model_width), jnp.bfloat16)
        .at[slot_index]
        .set(source_rows)
    )
    outgoing = outgoing.reshape(expert_count, capacity, model_width)
    gate_local_w = w_gate[0]
    up_local_weight = w_up[0]
    down_local_w = w_down[0]
    arrived = lax.all_to_all(outgoing, "sp", split_axis=0, concat_axis=0, tiled=True)
    slot_count = arrived.shape[1]
    sources = arrived.shape[0]
    pooled = lax.all_gather(arrived, "tp", axis=0, tiled=True)
    row_count = lax.axis_size("tp") * sources
    picked = pooled.reshape(row_count * slot_count, model_width)
    gate_act = jnp.dot(picked, gate_local_w, preferred_element_type=jnp.float32)
    up_act = jnp.dot(picked, up_local_weight, preferred_element_type=jnp.float32)
    activated = (jax.nn.silu(gate_act) * up_act).astype(jnp.bfloat16)
    result = jnp.dot(activated, down_local_w, preferred_element_type=jnp.float32)
    summed = lax.psum_scatter(
        result.reshape(row_count, slot_count, model_width).astype(jnp.bfloat16),
        "tp",
        scatter_dimension=0,
        tiled=True,
    )
    returned = lax.all_to_all(summed, "sp", split_axis=0, concat_axis=0, tiled=True)
    fetched = returned.reshape(expert_count * capacity, model_width)[slot_index]
    fetched = fetched.astype(jnp.float32).reshape(tok_row, top_count, model_width)
    mixture = jnp.sum(route_weight[:, :, None] * fetched, axis=1)
    return (stream + mixture).astype(jnp.bfloat16)


def solution(mesh):
    return jax.shard_map(
        shards,
        mesh=mesh,
        in_specs=(
            P("sp", "tp"),
            P("sp", "tp"),
            P("sp", "tp"),
            P("sp", "tp"),
            P(("sp", "tp"), None),
            P(),
            P(),
            P(("sp", "tp"), None),
            P(("sp", "tp"), None),
            P("sp", None, "tp"),
            P("sp", None, "tp"),
            P("sp", "tp", None),
        ),
        out_specs=P(("sp", "tp"), None),
        check_vma=False,
    )
```

profile of v0, /device:TPU:0, one launch (start us, length us, event | category | flops | bytes accessed | tf_op | source)
XLA Modules:
  0.0 208.9 jit_solution(2447561701416402841)
XLA Ops:
  6.5 28.3 %all_gather.12 = bf16[1024,64]{0,1:T(8,128)(2,1)S(1)} all-gather(bf16[128,64]{0,1:T(8,128)(2,1)} %param.15), channel_id=1, replica_groups=mesh['sp'=8,'tp'=4] {'sp'}, dimensions={0}, use_global_device_ids=true | all-gather | bytes 147456 | tf_op jit(solution)/shard_map/all_gather | solution.py:74
  34.8 26.4 %all_gather.14 = bf16[1024,64]{0,1:T(8,128)(2,1)S(1)} all-gather(bf16[128,64]{0,1:T(8,128)(2,1)} %param.16), channel_id=1, replica_groups=mesh['sp'=8,'tp'=4] {'sp'}, dimensions={0}, use_global_device_ids=true | all-gather | bytes 147456 | tf_op jit(solution)/shard_map/all_gather | solution.py:75
  61.2 26.2 %all_gather.13 = f32[1024,4]{0,1:T(4,128)S(1)} all-gather(f32[128,4]{0,1:T(4,128)} %param.17), channel_id=1, replica_groups=mesh['sp'=8,'tp'=4] {'sp'}, dimensions={0}, use_global_device_ids=true | all-gather | bytes 18432 | tf_op jit(solution)/shard_map/all_gather | solution.py:37
  87.5 3.4 %conditional.1 = ((f32[1,4,128]{2,1,0:T(4,128)S(1)}, f32[128,1,4,64]{0,3,2,1:T(8,128)S(1)})) conditional(s32[]{:T(128)} %convert_element_type.38, (f32[1,4,128]{2,1,0:T(4,128)S(1)}, f32[128,1,4,64]{0,3,2,1:T(8,128)S(1)}) %tuple.22, (s32[]{:T(128)}, s32[128]{0:T(128)S(1)}, bf16[128,256]{1,0:T(8,128)(2,1)}, bf16[1024,64]{0,1:T(8,128)(2,1)S(1)}, ...), branch_computations={%region_0.1_spmd, %region_1.4_spmd} | conditional | flops 140183680 | bytes 7581212 | solution.py:83
  87.6 1.0 copy.27
  88.6 1.4 fusion.25
  90.0 0.5 fusion.4
  90.5 0.4 fusion.3
  91.1 0.8 all_to_all.20
  91.9 3.3 %all-to-all-start = ((bf16[4,32,256]{2,1,0:T(8,128)(2,1)}), bf16[4,32,256]{2,1,0:T(8,128)(2,1)S(1)}, u32[]{:S(2)}, u32[]{:S(2)}) async-start(bf16[4,32,256]{2,1,0:T(8,128)(2,1)} %all_to_all.20), calls=%async_computation | async-start | bytes 131072 | tf_op jit(solution)/shard_map/all_to_all | solution.py:95
  96.0 3.2 %all-to-all-done = bf16[4,32,256]{2,1,0:T(8,128)(2,1)S(1)} async-done(((bf16[4,32,256]{2,1,0:T(8,128)(2,1)}), bf16[4,32,256]{2,1,0:T(8,128)(2,1)S(1)}, u32[]{:S(2)}, u32[]{:S(2)}) %all-to-all-start) | async-done | bytes 65568 | tf_op jit(solution)/shard_map/all_to_all | solution.py:95
  99.3 3.1 %multiply_reduce_fusion.1 = (f32[32]{0:T(128)S(1)}, f32[32,2048]{1,0:T(8,128)S(1)}) fusion(bf16[32,1024]{1,0:T(8,128)(2,1)S(1)} %bitcast.86, bf16[1024,2048]{1,0:T(8,128)(2,1)} %param.19, bf16[32,2048]{1,0:T(8,128)(2,1)S(1)} %copy-done.1), kind=kOutput, calls=%fused_computation.38 | convolution fusion | flops 134479840 | bytes 4653184 | tf_op jit(solution)/shard_map/dot_general | solution.py:96
  102.5 2.0 scatter_custom_fusion
  104.5 17.7 %all_to_all.29 = bf16[8,16,2048]{2,1,0:T(8,128)(2,1)} all-to-all(bf16[8,16,2048]{2,1,0:T(8,128)(2,1)S(1)} %bitcast.85), channel_id=1, replica_groups=mesh['sp'=8,'tp'=4] {'sp'}, dimensions={0} | all-to-all | bytes 1048576 | tf_op jit(solution)/shard_map/all_to_all | solution.py:120
  122.3 20.8 %all-gather.2.cloned.1.call-done = bf16[32,16,2048]{2,1,0:T(8,128)(2,1)} async-done(((bf16[8,16,2048]{2,1,0:T(8,128)(2,1)}), bf16[32,16,2048]{2,1,0:T(8,128)(2,1)}) %all-gather.2.cloned.1.call-update) | async-done | bytes 2097168 | tf_op jit(solution)/shard_map/all_gather | solution.py:123
  143.1 2.5 %fusion.17 = f32[512,256]{1,0:T(8,128)S(1)} fusion(bf16[512,2048]{1,0:T(8,128)(2,1)} %bitcast.94, bf16[1,2048,256]{2,1,0:T(8,128)(2,1)S(1)} %copy-done.6), kind=kOutput, calls=%fused_computation.31 | convolution fusion | flops 536870912 | bytes 3670016 | tf_op jit(solution)/shard_map/dot_general | solution.py:126
  145.5 0.7 fusion.14
  146.3 2.1 convolution_convert_fusion
  148.4 31.3 %reduce-scatter.2.cloned.1.call-done = bf16[8,16,2048]{2,1,0:T(8,128)(2,1)} async-done(((bf16[32,16,2048]{2,1,0:T(8,128)(2,1)}), bf16[8,16,2048]{2,1,0:T(8,128)(2,1)}) %reduce-scatter.2.cloned.1.call-update) | async-done | bytes 524304 | tf_op jit(solution)/shard_map/reduce_scatter | solution.py:130
  179.7 5.5 %all-to-all-start.2 = ((bf16[8,16,2048]{2,1,0:T(8,128)(2,1)}), bf16[8,16,2048]{2,1,0:T(8,128)(2,1)S(1)}, u32[]{:S(2)}, u32[]{:S(2)}) async-start(bf16[8,16,2048]{2,1,0:T(8,128)(2,1)} %reduce-scatter.2.cloned.1.call-done), calls=%async_computation.3 | async-start | bytes 1048576 | tf_op jit(solution)/shard_map/all_to_all | solution.py:136
  185.3 14.2 %all-to-all-done.2 = bf16[8,16,2048]{2,1,0:T(8,128)(2,1)S(1)} async-done(((bf16[8,16,2048]{2,1,0:T(8,128)(2,1)}), bf16[8,16,2048]{2,1,0:T(8,128)(2,1)S(1)}, u32[]{:S(2)}, u32[]{:S(2)}) %all-to-all-start.2) | async-done | bytes 524320 | tf_op jit(solution)/shard_map/all_to_all | solution.py:136
  199.5 0.7 gather_fusion
  200.6 0.7 multiply_reduce_fusion
  201.4 0.7 add_convert_fusion
  (46 shorter events, 1.8 us)
Async XLA Ops:
  6.5 139.7 %copy-start = (bf16[1,256,2048]{2,1,0:T(8,128)(2,1)S(1)}, bf16[1,256,2048]{2,1,0:T(8,128)(2,1)}, u32[]{:S(2)}) copy-start(bf16[1,256,2048]{2,1,0:T(8,128)(2,1)} %param.25) | copy-start | bytes 3145732
  87.5 7.7 %copy-start.3 = (s32[32,2]{0,1:T(2,128)S(1)}, s32[32,2]{0,1:T(2,128)}, u32[]{:S(2)}) copy-start(s32[32,2]{0,1:T(2,128)} %param.21) | copy-start | bytes 772
  87.5 11.7 %copy-start.1 = (bf16[32,2048]{1,0:T(8,128)(2,1)S(1)}, bf16[32,2048]{1,0:T(8,128)(2,1)}, u32[]{:S(2)}) copy-start(bf16[32,2048]{1,0:T(8,128)(2,1)} %param.18) | copy-start | bytes 393220
  91.9 7.4 %all-to-all-start = ((bf16[4,32,256]{2,1,0:T(8,128)(2,1)}), bf16[4,32,256]{2,1,0:T(8,128)(2,1)S(1)}, u32[]{:S(2)}, u32[]{:S(2)}) async-start(bf16[4,32,256]{2,1,0:T(8,128)(2,1)} %all_to_all.20), calls=%async_computation | async-start | bytes 131072 | tf_op jit(solution)/shard_map/all_to_all | solution.py:95
  95.1 47.9 %all-gather.2.cloned.1.call-start = ((), (), s32[]{:S(2)}) async-start(), calls=%async_computation.4 | async-start | bytes 2621440 | tf_op jit(solution)/shard_map/all_gather | solution.py:123
  99.2 3.2 %copy-start.2 = (f32[2048]{0:T(1024)S(1)}, f32[2048]{0:T(1024)}, u32[]{:S(2)}) copy-start(f32[2048]{0:T(1024)} %param.20) | copy-start | bytes 24580
  102.4 40.7 %copy-start.6 = (bf16[1,2048,256]{2,1,0:T(8,128)(2,1)S(1)}, bf16[1,2048,256]{2,1,0:T(8,128)(2,1)}, u32[]{:S(2)}) copy-start(bf16[1,2048,256]{2,1,0:T(8,128)(2,1)} %param.23) | copy-start | bytes 3145732
  122.2 23.3 %copy-start.7 = (bf16[1,2048,256]{2,1,0:T(8,128)(2,1)S(1)}, bf16[1,2048,256]{2,1,0:T(8,128)(2,1)}, u32[]{:S(2)}) copy-start(bf16[1,2048,256]{2,1,0:T(8,128)(2,1)} %param.24) | copy-start | bytes 3145732
  122.2 57.5 %reduce-scatter.2.cloned.1.call-start = ((), (), s32[]{:S(2)}) async-start(), calls=%async_computation.5 | async-start | bytes 2621440 | tf_op jit(solution)/shard_map/reduce_scatter | solution.py:130
  143.0 2.5 %copy-start.5 = (bf16[32,16,2048]{2,1,0:T(8,128)(2,1)S(1)}, bf16[32,16,2048]{2,1,0:T(8,128)(2,1)}, u32[]{:S(2)}) copy-start(bf16[32,16,2048]{2,1,0:T(8,128)(2,1)} %all-gather.2.cloned.1.call-done) | copy-start | bytes 6291460
  148.3 36.9 %copy-start.4 = (f32[32,2]{0,1:T(2,128)S(1)}, f32[32,2]{0,1:T(2,128)}, u32[]{:S(2)}) copy-start(f32[32,2]{0,1:T(2,128)} %param.22) | copy-start | bytes 772
  179.7 19.8 %all-to-all-start.2 = ((bf16[8,16,2048]{2,1,0:T(8,128)(2,1)}), bf16[8,16,2048]{2,1,0:T(8,128)(2,1)S(1)}, u32[]{:S(2)}, u32[]{:S(2)}) async-start(bf16[8,16,2048]{2,1,0:T(8,128)(2,1)} %reduce-scatter.2.cloned.1.call-done), calls=%async_computation.3 | async-start | bytes 1048576 | tf_op jit(solution)/shard_map/all_to_all | solution.py:136
Sparse Core Ops, SparseCore 0:
  122.3 20.6 all-gather.1
  148.5 31.1 reduce-scatter.1
where the time goes:
time: 209 us
  blocking collectives  98.6 us (47%)
  waiting for transfers between devices  69.6 us (33%)
  between operations  13.6 us (7%)
  matrix products  10.3 us (5%)
  starting transfers between devices  8.88 us (4%)
  local copies, waits for them, and re-layouts  5.46 us (3%)
  other arithmetic  2.43 us (1%)
    reduce_scatter x1, waiting for transfers between devices, shards(): lax.psum_scatter(result.reshape(row_count, slot_count, model_width).astyp...  31.3 us
    all_gather x1, blocking collectives, shards(): key_piece = lax.all_gather(keys, 'sp', axis=0, tiled=True)  28.3 us
    all_gather x1, blocking collectives, shards(): value_piece = lax.all_gather(values, 'sp', axis=0, tiled=True)  26.4 us
    all_gather x1, blocking collectives, shards(): gates_all = lax.all_gather(forget_prefix_log, 'sp', axis=0, tiled=True)  26.2 us
    all_gather x1, waiting for transfers between devices, shards(): pooled = lax.all_gather(arrived, 'tp', axis=0, tiled=True)  20.8 us
    all_to_all x1, blocking collectives, shards(): lax.all_to_all(outgoing, 'sp', split_axis=0, concat_axis=0, tiled=True)  17.7 us
    all_to_all x1, waiting for transfers between devices, shards(): lax.all_to_all(summed, 'sp', split_axis=0, concat_axis=0, tiled=True)  14.2 us
    all_to_all x1, starting transfers between devices, shards(): lax.all_to_all(summed, 'sp', split_axis=0, concat_axis=0, tiled=True)  5.52 us
  transfers between devices with their start and end apart: 4, of which 4 were waited for; matrix products, arithmetic and copies ran while one was open for 0% of the time, Pallas kernels for 0%

commit v1 on v0

v1 whole, which is shorter than its diff:
```python
import functools

import jax
import jax.numpy as jnp
from jax import lax
from jax.experimental import pallas as pl
from jax.experimental.pallas import tpu as pltpu
from jax.sharding import PartitionSpec as P

HEAD_DIM = 64
MESH = pl.DeviceIdType.MESH
F32 = jnp.float32
BF16 = jnp.bfloat16


def each(first, last, body):
    def step(i, carry):
        body(i)
        return carry

    lax.fori_loop(first, last, step, 0)


def layer_kernel(
    n_sp,
    n_tp,
    q_ref,
    kv_ref,
    gate_ref,
    residual_ref,
    gain_ref,
    routes_ref,
    routes_t_ref,
    route_weight_ref,
    ow_hbm,
    wg_hbm,
    wu_hbm,
    wd_hbm,
    out_ref,
    kv_all,
    gate_all,
    attended,
    swapped,
    stream,
    ow,
    wg,
    wu,
    wd,
    outgoing,
    pool,
    core_part,
    x_stage,
    x_part,
    back_stage,
    back,
    kept,
    kept_own,
    local_sem,
    kv_sem,
    gate_sem,
    swap_sem,
    disp_sem,
    xf_sem,
    cf_sem,
    cf2_sem,
    core_sem,
    x_sem,
    ret_sem,
):
    s = lax.axis_index("sp")
    t = lax.axis_index("tp")
    t_core = t + 1 - 2 * lax.rem(t, 2)
    t_x = t + 2 - 4 * lax.rem(lax.div(t, 2), 2)
    tok = q_ref.shape[0]
    heads = gate_ref.shape[0]
    tok_row, width = residual_ref.shape
    capp = outgoing.shape[1]
    slots = n_sp * capp
    head_cols = heads * HEAD_DIM

    def remote(src, dst, sems, index, to):
        return pltpu.make_async_remote_copy(
            src_ref=src,
            dst_ref=dst,
            send_sem=sems.at[0, index],
            recv_sem=sems.at[1, index],
            device_id=to,
            device_id_type=MESH,
        )

    loads = [
        pltpu.make_async_copy(a, b, local_sem.at[i])
        for i, (a, b) in enumerate(
            [(ow_hbm, ow), (wg_hbm.at[0], wg), (wu_hbm.at[0], wu), (wd_hbm.at[0], wd)]
        )
    ]
    for load in loads:
        load.start()

    barrier = pltpu.get_barrier_semaphore()

    def greet_sp(d):
        pl.semaphore_signal(
            barrier, inc=1, device_id=(lax.rem(s + d, n_sp), t), device_id_type=MESH
        )

    def greet_tp(k):
        pl.semaphore_signal(
            barrier, inc=1, device_id=(s, lax.rem(t + k, n_tp)), device_id_type=MESH
        )

    each(1, n_sp, greet_sp)
    each(1, n_tp, greet_tp)
    pl.semaphore_wait(barrier, n_sp - 1 + n_tp - 1)

    def kv_copy(d):
        return remote(kv_ref, kv_all.at[d], kv_sem, d, (lax.rem(s + d, n_sp), t))

    def gate_copy(d):
        return remote(gate_ref, gate_all.at[d], gate_sem, d, (lax.rem(s + d, n_sp), t))

    def send_kv(d):
        kv_copy(d).start()
        gate_copy(d).start()

    each(1, n_sp - s, send_kv)

    rows_i = lax.broadcasted_iota(jnp.int32, (tok_row, tok_row), 0)
    cols_i = lax.broadcasted_iota(jnp.int32, (tok_row, tok_row), 1)
    top = routes_ref.shape[1]
    col = [routes_ref[:, k : k + 1] for k in range(top)]
    row = [routes_t_ref[k : k + 1, :] for k in range(top)]
    slot_row, slot_col = [], []
    for k in range(top):
        rank_row = jnp.zeros((1, tok_row), F32)
        rank_col = jnp.zeros((tok_row, 1), F32)
        for other in range(top):
            same = jnp.logical_and(col[other] == row[k], rows_i < cols_i)
            rank_row = rank_row + jnp.sum(jnp.where(same, 1.0, 0.0), axis=0, keepdims=True)
            same = jnp.logical_and(row[other] == col[k], cols_i < rows_i)
            rank_col = rank_col + jnp.sum(jnp.where(same, 1.0, 0.0), axis=1, keepdims=True)
        slot_row.append((lax.rem(row[k] - s + n_sp, n_sp) * capp).astype(F32) + rank_row)
        slot_col.append((lax.rem(col[k] - s + n_sp, n_sp) * capp).astype(F32) + rank_col)
    slot_of_row = lax.broadcasted_iota(jnp.int32, (slots, tok_row), 0).astype(F32)
    slot_of_col = lax.broadcasted_iota(jnp.int32, (tok_row, slots), 1).astype(F32)
    spread = jnp.zeros((slots, tok_row), F32)
    for k in range(top):
        spread = spread + jnp.where(slot_of_row == slot_row[k], 1.0, 0.0)
    spread = spread.astype(BF16)

    query = q_ref[...] * jnp.asarray(HEAD_DIM**-0.5, BF16)
    stacked = jnp.concatenate(
        [query[:, h * HEAD_DIM : (h + 1) * HEAD_DIM] for h in range(heads)], axis=0
    )

    def scores_of(kv, gate):
        raw = lax.dot_general(
            stacked,
            kv[:, :HEAD_DIM],
            (((1,), (1,)), ((), ())),
            preferred_element_type=F32,
        )
        return raw.reshape(heads, tok, tok) - gate[:, None, :]

    def weigh(weights, kv):
        return jnp.dot(
            weights.astype(BF16).reshape(heads * tok, tok),
            kv[:, HEAD_DIM:],
            preferred_element_type=F32,
        ).reshape(heads, tok, HEAD_DIM)

    kv_own = kv_ref[...]
    scores = scores_of(kv_own, gate_ref[...])
    causal = lax.broadcasted_iota(jnp.int32, (heads, tok, tok), 1) >= lax.broadcasted_iota(
        jnp.int32, (heads, tok, tok), 2
    )
    scores = jnp.where(causal, scores, -1e30)
    peak = jnp.max(scores, axis=-1, keepdims=True)
    weights = jnp.exp(scores - peak)
    total = jnp.sum(weights, axis=-1, keepdims=True)
    weighted = weigh(weights, kv_own)

    def absorb(d, state):
        peak, total, weighted = state
        kv_copy(d).wait_recv()
        gate_copy(d).wait_recv()
        kv = kv_all[d]
        scores = scores_of(kv, gate_all[d])
        new_peak = jnp.maximum(peak, jnp.max(scores, axis=-1, keepdims=True))
        weights = jnp.exp(scores - new_peak)
        shrink = jnp.exp(peak - new_peak)
        total = total * shrink + jnp.sum(weights, axis=-1, keepdims=True)
        weighted = weighted * shrink + weigh(weights, kv)
        return new_peak, total, weighted

    peak, total, weighted = lax.fori_loop(1, s + 1, absorb, (peak, total, weighted))
    result = (weighted / total).astype(BF16)
    for h in range(heads):
        attended[:, h * HEAD_DIM : (h + 1) * HEAD_DIM] = result[h]

    def rows_of(p):
        return pl.ds(pl.multiple_of(p * tok_row, tok_row), tok_row)

    def swap_copy(k):
        p = lax.rem(t + k, n_tp)
        return remote(attended.at[rows_of(p)], swapped.at[k], swap_sem, k, (s, p))

    for k in range(1, n_tp):
        swap_copy(k).start()
    loads[0].wait()

    def weight_rows(p):
        return ow[pl.ds(pl.multiple_of(p * head_cols, head_cols), head_cols), :]

    total_stream = residual_ref[...].astype(F32) + jnp.dot(
        attended[rows_of(t), :], weight_rows(t), preferred_element_type=F32
    )
    for k in range(1, n_tp):
        swap_copy(k).wait_recv()
        total_stream = total_stream + jnp.dot(
            swapped[k], weight_rows(lax.rem(t - k + n_tp, n_tp)), preferred_element_type=F32
        )
    stream[...] = total_stream
    mean_square = jnp.mean(total_stream * total_stream, axis=-1, keepdims=True)
    normed = (total_stream * lax.rsqrt(mean_square + 1e-06) * gain_ref[...]).astype(BF16)

    dispatched = jnp.dot(spread, normed, preferred_element_type=F32).astype(BF16)
    outgoing[...] = dispatched.reshape(n_sp, capp, width)
    pool[0, 0] = dispatched[:capp]

    def disp_copy(d):
        return remote(
            outgoing.at[d], pool.at[d, 0], disp_sem, d, (lax.rem(s + d, n_sp), t)
        )

    each(1, n_sp, lambda d: disp_copy(d).start())

    def xf_copy(d):
        return remote(pool.at[d, 0], pool.at[d, 1], xf_sem, d, (s, t_x))

    def cf_copy(d):
        return remote(pool.at[d, 0], pool.at[d, 2], cf_sem, d, (s, t_core))

    def cf2_copy(d):
        return remote(pool.at[d, 1], pool.at[d, 3], cf2_sem, d, (s, t_core))

    def core_copy(d):
        return remote(pool.at[d, pl.ds(2, 2)], core_part.at[d], core_sem, d, (s, t_core))

    def x_copy(d):
        return remote(x_stage.at[d], x_part.at[d], x_sem, d, (s, t_x))

    def ret_copy(d):
        return remote(
            back_stage.at[d], back.at[d], ret_sem, d, (lax.rem(s - d + n_sp, n_sp), t)
        )

    for load in loads[1:]:
        load.wait()

    def stage(i, lag, body):
        d = i - lag

        @pl.when(jnp.logical_and(d >= 0, d < n_sp))
        def _():
            body(d)

    def arrive(d):
        @pl.when(d > 0)
        def _():
            disp_copy(d).wait_recv()

        xf_copy(d).start()
        cf_copy(d).start()

    def relay(d):
        xf_copy(d).wait_recv()
        cf2_copy(d).start()

    def compute(d):
        cf_copy(d).wait_recv()
        cf2_copy(d).wait_recv()
        picked = pool[d].reshape(4 * capp, width)
        gate_act = jnp.dot(picked, wg[...], preferred_element_type=F32)
        up_act = jnp.dot(picked, wu[...], preferred_element_type=F32)
        hidden = (gate_act / (1.0 + jnp.exp(-gate_act)) * up_act).astype(BF16)
        part = jnp.dot(hidden, wd[...], preferred_element_type=F32)
        pool[d, pl.ds(2, 2)] = part[2 * capp :].astype(BF16).reshape(2, capp, width)
        kept[lax.rem(d, 2)] = part[: 2 * capp]
        core_copy(d).start()

    def over_cores(d):
        core_copy(d).wait_recv()
        both = kept[lax.rem(d, 2)] + core_part[d].reshape(2 * capp, width).astype(F32)
        x_stage[d] = both[capp:].astype(BF16)
        kept_own[lax.rem(d, 2)] = both[:capp]
        x_copy(d).start()

    def over_x(d):
        x_copy(d).wait_recv()
        done = (kept_own[lax.rem(d, 2)] + x_part[d].astype(F32)).astype(BF16)

        @pl.when(d == 0)
        def _():
            back[0] = done

        @pl.when(d > 0)
        def _():
            back_stage[d] = done
            ret_copy(d).start()

    def pipeline(i):
        stage(i, 0, arrive)
        stage(i, 1, relay)
        stage(i, 4, over_x)
        stage(i, 3, over_cores)
        stage(i, 2, compute)

    each(0, n_sp + 4, pipeline)

    combine = jnp.zeros((tok_row, slots), F32)
    for k in range(top):
        combine = combine + jnp.where(
            slot_of_col == slot_col[k], route_weight_ref[:, k : k + 1], 0.0
        )
    high = combine.astype(BF16)
    low = (combine - high.astype(F32)).astype(BF16)
    each(1, n_sp, lambda d: ret_copy(d).wait_recv())
    returned = back[...].reshape(slots, width)
    mixture = jnp.dot(high, returned, preferred_element_type=F32) + jnp.dot(
        low, returned, preferred_element_type=F32
    )
    out_ref[...] = (stream[...] + mixture).astype(out_ref.dtype)

    def sent_kv(d):
        kv_copy(d).wait_send()
        gate_copy(d).wait_send()

    each(1, n_sp - s, sent_kv)
    for k in range(1, n_tp):
        swap_copy(k).wait_send()

    def sent(d):
        @pl.when(d > 0)
        def _():
            disp_copy(d).wait_send()
            ret_copy(d).wait_send()

        for copy in (xf_copy, cf_copy, cf2_copy, core_copy, x_copy):
            copy(d).wait_send()

    each(0, n_sp, sent)


def shards(
    n_sp,
    n_tp,
    queries,
    keys,
    values,
    forget_prefix_log,
    residual,
    out_weight,
    norm_gain,
    routes,
    route_weight,
    w_gate,
    w_up,
    w_down,
):
    tok = queries.shape[0]
    heads = forget_prefix_log.shape[1]
    assert keys.shape[1] == HEAD_DIM and n_tp == 4
    tok_row, width = residual.shape
    capacity = max(2, 2 * tok_row * routes.shape[1] // n_sp)
    capp = -(-capacity // 16) * 16
    quarter = w_gate.shape[2]
    kv = jnp.concatenate([keys, values], axis=1)
    vmem = pl.BlockSpec(memory_space=pltpu.VMEM)
    hbm = pl.BlockSpec(memory_space=pl.ANY)
    sems = lambda n: pltpu.SemaphoreType.DMA((2, n))
    block = (n_sp, capp, width)
    return pl.pallas_call(
        functools.partial(layer_kernel, n_sp, n_tp),
        out_shape=jax.ShapeDtypeStruct((tok_row, width), BF16),
        in_specs=[vmem] * 8 + [hbm] * 4,
        out_specs=vmem,
        scratch_shapes=[
            pltpu.VMEM((n_sp, tok, 2 * HEAD_DIM), BF16),
            pltpu.VMEM((n_sp, heads, tok), F32),
            pltpu.VMEM((tok, heads * HEAD_DIM), BF16),
            pltpu.VMEM((n_tp, tok_row, heads * HEAD_DIM), BF16),
            pltpu.VMEM((tok_row, width), F32),
            pltpu.VMEM(out_weight.shape, BF16),
            pltpu.VMEM((width, quarter), BF16),
            pltpu.VMEM((width, quarter), BF16),
            pltpu.VMEM((quarter, width), BF16),
            pltpu.VMEM(block, BF16),
            pltpu.VMEM((n_sp, 4, capp, width), BF16),
            pltpu.VMEM((n_sp, 2, capp, width), BF16),
            pltpu.VMEM(block, BF16),
            pltpu.VMEM(block, BF16),
            pltpu.VMEM(block, BF16),
            pltpu.VMEM(block, BF16),
            pltpu.VMEM((2, 2 * capp, width), F32),
            pltpu.VMEM((2, capp, width), F32),
            pltpu.SemaphoreType.DMA((4,)),
            sems(n_sp),
            sems(n_sp),
            sems(n_tp),
            sems(n_sp),
            sems(n_sp),
            sems(n_sp),
            sems(n_sp),
            sems(n_sp),
            sems(n_sp),
            sems(n_sp),
        ],
        compiler_params=pltpu.CompilerParams(
            collective_id=0, has_side_effects=True, vmem_limit_bytes=66_000_000
        ),
    )(
        queries,
        kv,
        forget_prefix_log.T,
        residual,
        norm_gain.reshape(1, width),
        routes,
        routes.T,
        route_weight,
        out_weight,
        w_gate,
        w_up,
        w_down,
    )


def solution(mesh):
    return jax.shard_map(
        functools.partial(shards, mesh.shape["sp"], mesh.shape["tp"]),
        mesh=mesh,
        in_specs=(
            P("sp", "tp"),
            P("sp", "tp"),
            P("sp", "tp"),
            P("sp", "tp"),
            P(("sp", "tp"), None),
            P(),
            P(),
            P(("sp", "tp"), None),
            P(("sp", "tp"), None),
            P("sp", None, "tp"),
            P("sp", None, "tp"),
            P("sp", "tp", None),
        ),
        out_specs=P(("sp", "tp"), None),
        check_vma=False,
    )
```

time: 209 us -> 72.5 us (0.35)
  blocking collectives: 98.6 us -> 0 us
  waiting for transfers between devices: 69.6 us -> 0 us
  Pallas kernels: 0 us -> 65.4 us
  between operations: 13.6 us -> 0.01 us
  matrix products: 10.3 us -> 0 us
  starting transfers between devices: 8.88 us -> 0 us
    all_gather x3 -> x0, blocking collectives: 80.9 us -> none  [the longest x1 28.3 us: shards(): key_piece = lax.all_gather(keys, 'sp', axis=0, tiled=True)]
    pallas_call x0 -> x1, Pallas kernels: none -> 65.4 us  [shards(): pl.pallas_call(functools.partial(layer_kernel, n_sp, n_tp), out_shape=jax...]
    reduce_scatter x1 -> x0, waiting for transfers between devices: 31.3 us -> none  [shards(): lax.psum_scatter(result.reshape(row_count, slot_count, model_width).astyp...]
    all_gather x1 -> x0, waiting for transfers between devices: 20.8 us -> none  [shards(): pooled = lax.all_gather(arrived, 'tp', axis=0, tiled=True)]
    all_to_all x1 -> x0, blocking collectives: 17.7 us -> none  [shards(): lax.all_to_all(outgoing, 'sp', split_axis=0, concat_axis=0, tiled=True)]
    all_to_all x2 -> x0, waiting for transfers between devices: 17.5 us -> none  [the longest x1 14.2 us: shards(): lax.all_to_all(summed, 'sp', split_axis=0, concat_axis=0, tiled=True)]
    dot_general x6 -> x0, matrix products: 10.3 us -> none  [the longest x1 3.13 us: shards(): projected = jnp.dot(swapped, out_weight, preferred_element_type=jnp.float32)]
    all_to_all x2 -> x0, starting transfers between devices: 8.8 us -> none  [the longest x1 5.52 us: shards(): lax.all_to_all(summed, 'sp', split_axis=0, concat_axis=0, tiled=True)]
  transfers between devices with their start and end apart: 4 -> 0, of which waited for: 4 -> 0; matrix products, arithmetic and copies ran while one was open for 0% -> 0% of each run, Pallas kernels for 0% -> 0%
where the time goes in v1:
time: 72.5 us; the launch traced here: 72.1 us
  Pallas kernels  65.4 us (90%)
  local copies, waits for them, and re-layouts  5.93 us (8%)
    pallas_call x1, Pallas kernels, shards(): pl.pallas_call(functools.partial(layer_kernel, n_sp, n_tp), out_shape=jax...  65.4 us
    unnamed x5, local copies, waits for them, and re-layouts  5.93 us

profile of v1, /device:TPU:0, one launch (start us, length us, event | category | flops | bytes accessed | tf_op | source)
XLA Modules:
  0.0 72.1 jit_solution(24053464635042919)
XLA Ops:
  0.0 1.4 %copy.16.route_weight_ref = f32[32,2]{1,0:T(8,128)} copy(f32[32,2]{0,1:T(2,128)} %param.20) | data formatting | bytes 512 | tf_op args[8]
  1.4 1.4 %copy.15.routes_ref = s32[32,2]{1,0:T(8,128)} copy(s32[32,2]{0,1:T(2,128)} %param.19) | data formatting | bytes 512 | tf_op args[7]
  2.7 0.8 %copy.13 = bf16[128,64]{1,0:T(8,128)(2,1)S(1)} copy(bf16[128,64]{0,1:T(8,128)(2,1)} %param.13) | data formatting | bytes 32768 | tf_op args[1]
  3.5 0.8 %copy.14 = bf16[128,64]{1,0:T(8,128)(2,1)S(1)} copy(bf16[128,64]{0,1:T(8,128)(2,1)} %param.14) | data formatting | bytes 32768 | tf_op args[2]
  4.4 0.7 pad_maximum_fusion.kv_ref
  5.1 65.4 %shard_map.118 = bf16[32,2048]{1,0:T(8,128)(2,1)} custom-call(bf16[128,256]{1,0:T(8,128)(2,1)} %q_ref.1, bf16[128,128]{1,0:T(8,128)(2,1)} %pad_maximum_fusion.kv_ref, f32[4,128]{1,0:T(4,128)} %bitcast.5, bf16[32,2048]{1,0:T(8,128)(2,1)} %residual_ref.1, f32[1,2048]{1,0:T(1,128)} %bitcast.3, s32[32,2]{1,0:T(8,128)} %copy.15.routes_ref, s32[2,32]{1,0:T(2,128)} %bitcast.4, ...), custom_call_target="tpu_custom_call" | custom-call | tf_op jit(solution)/shard_map/pallas_call | solution.py:383
  70.5 1.6 %copy.18 = bf16[32,2048]{1,0:T(8,128)(2,1)} copy(bf16[32,2048]{1,0:T(8,128)(2,1)} %shard_map.118) | data formatting | bytes 262144

commit v2 on v1

--- a/solution.py
+++ b/solution.py
@@ -25,12 +25,12 @@
     n_sp,
     n_tp,
     q_ref,
-    kv_ref,
+    key_ref,
+    value_ref,
     gate_ref,
     residual_ref,
     gain_ref,
     routes_ref,
-    routes_t_ref,
     route_weight_ref,
     ow_hbm,
     wg_hbm,
@@ -49,14 +49,11 @@
     outgoing,
     pool,
     core_part,
-    x_stage,
     x_part,
-    back_stage,
     back,
-    kept,
-    kept_own,
     local_sem,
-    kv_sem,
+    key_sem,
+    value_sem,
     gate_sem,
     swap_sem,
     disp_sem,
@@ -78,6 +75,13 @@
     slots = n_sp * capp
     head_cols = heads * HEAD_DIM
 
+    def partner(a, b):
+        both, bit = 0, 1
+        while bit < n_sp:
+            both = both + bit * (lax.rem(lax.div(a, bit), 2) * lax.rem(lax.div(b, bit), 2))
+            bit *= 2
+        return a + b - 2 * both
+
     def remote(src, dst, sems, index, to):
         return pltpu.make_async_remote_copy(
             src_ref=src,
@@ -113,34 +117,37 @@
     each(1, n_tp, greet_tp)
     pl.semaphore_wait(barrier, n_sp - 1 + n_tp - 1)
 
-    def kv_copy(d):
-        return remote(kv_ref, kv_all.at[d], kv_sem, d, (lax.rem(s + d, n_sp), t))
-
-    def gate_copy(d):
-        return remote(gate_ref, gate_all.at[d], gate_sem, d, (lax.rem(s + d, n_sp), t))
+    def kv_copies(d):
+        to = (lax.rem(s + d, n_sp), t)
+        return (
+            remote(key_ref, kv_all.at[d, pl.ds(0, HEAD_DIM)], key_sem, d, to),
+            remote(value_ref, kv_all.at[d, pl.ds(HEAD_DIM, HEAD_DIM)], value_sem, d, to),
+            remote(gate_ref, gate_all.at[d], gate_sem, d, to),
+        )
 
     def send_kv(d):
-        kv_copy(d).start()
-        gate_copy(d).start()
+        for copy in kv_copies(d):
+            copy.start()
 
     each(1, n_sp - s, send_kv)
 
     rows_i = lax.broadcasted_iota(jnp.int32, (tok_row, tok_row), 0)
     cols_i = lax.broadcasted_iota(jnp.int32, (tok_row, tok_row), 1)
-    top = routes_ref.shape[1]
-    col = [routes_ref[:, k : k + 1] for k in range(top)]
-    row = [routes_t_ref[k : k + 1, :] for k in range(top)]
+    top = routes_ref.shape[0]
+    row = [routes_ref[k : k + 1, :] for k in range(top)]
+
+    def upright(line):
+        return jnp.sum(jnp.where(rows_i == cols_i, line, 0.0), axis=1, keepdims=True)
+
+    col = [upright(row[k].astype(F32)) for k in range(top)]
     slot_row, slot_col = [], []
     for k in range(top):
         rank_row = jnp.zeros((1, tok_row), F32)
-        rank_col = jnp.zeros((tok_row, 1), F32)
         for other in range(top):
-            same = jnp.logical_and(col[other] == row[k], rows_i < cols_i)
+            same = jnp.logical_and(col[other] == row[k].astype(F32), rows_i < cols_i)
             rank_row = rank_row + jnp.sum(jnp.where(same, 1.0, 0.0), axis=0, keepdims=True)
-            same = jnp.logical_and(row[other] == col[k], cols_i < rows_i)
-            rank_col = rank_col + jnp.sum(jnp.where(same, 1.0, 0.0), axis=1, keepdims=True)
-        slot_row.append((lax.rem(row[k] - s + n_sp, n_sp) * capp).astype(F32) + rank_row)
-        slot_col.append((lax.rem(col[k] - s + n_sp, n_sp) * capp).astype(F32) + rank_col)
+        slot_row.append((partner(row[k], s) * capp).astype(F32) + rank_row)
+        slot_col.append(upright(slot_row[k]))
     slot_of_row = lax.broadcasted_iota(jnp.int32, (slots, tok_row), 0).astype(F32)
     slot_of_col = lax.broadcasted_iota(jnp.int32, (tok_row, slots), 1).astype(F32)
     spread = jnp.zeros((slots, tok_row), F32)
@@ -153,24 +160,19 @@
         [query[:, h * HEAD_DIM : (h + 1) * HEAD_DIM] for h in range(heads)], axis=0
     )
 
-    def scores_of(kv, gate):
-        raw = lax.dot_general(
-            stacked,
-            kv[:, :HEAD_DIM],
+    def scores_of(key, gate):
+        raw = jnp.dot(stacked, key, preferred_element_type=F32)
+        return raw.reshape(heads, tok, tok) - gate[:, None, :]
+
+    def weigh(weights, value):
+        return lax.dot_general(
+            weights.astype(BF16).reshape(heads * tok, tok),
+            value,
             (((1,), (1,)), ((), ())),
             preferred_element_type=F32,
-        )
-        return raw.reshape(heads, tok, tok) - gate[:, None, :]
-
-    def weigh(weights, kv):
-        return jnp.dot(
-            weights.astype(BF16).reshape(heads * tok, tok),
-            kv[:, HEAD_DIM:],
-            preferred_element_type=F32,
         ).reshape(heads, tok, HEAD_DIM)
 
-    kv_own = kv_ref[...]
-    scores = scores_of(kv_own, gate_ref[...])
+    scores = scores_of(key_ref[...], gate_ref[...])
     causal = lax.broadcasted_iota(jnp.int32, (heads, tok, tok), 1) >= lax.broadcasted_iota(
         jnp.int32, (heads, tok, tok), 2
     )
@@ -178,19 +180,18 @@
     peak = jnp.max(scores, axis=-1, keepdims=True)
     weights = jnp.exp(scores - peak)
     total = jnp.sum(weights, axis=-1, keepdims=True)
-    weighted = weigh(weights, kv_own)
+    weighted = weigh(weights, value_ref[...])
 
     def absorb(d, state):
         peak, total, weighted = state
-        kv_copy(d).wait_recv()
-        gate_copy(d).wait_recv()
-        kv = kv_all[d]
-        scores = scores_of(kv, gate_all[d])
+        for copy in kv_copies(d):
+            copy.wait_recv()
+        scores = scores_of(kv_all[d, :HEAD_DIM], gate_all[d])
         new_peak = jnp.maximum(peak, jnp.max(scores, axis=-1, keepdims=True))
         weights = jnp.exp(scores - new_peak)
         shrink = jnp.exp(peak - new_peak)
         total = total * shrink + jnp.sum(weights, axis=-1, keepdims=True)
-        weighted = weighted * shrink + weigh(weights, kv)
+        weighted = weighted * shrink + weigh(weights, kv_all[d, HEAD_DIM:])
         return new_peak, total, weighted
 
     peak, total, weighted = lax.fori_loop(1, s + 1, absorb, (peak, total, weighted))
@@ -230,7 +231,7 @@
 
     def disp_copy(d):
         return remote(
-            outgoing.at[d], pool.at[d, 0], disp_sem, d, (lax.rem(s + d, n_sp), t)
+            outgoing.at[d], pool.at[d, 0], disp_sem, d, (partner(s, d), t)
         )
 
     each(1, n_sp, lambda d: disp_copy(d).start())
@@ -248,11 +249,11 @@
         return remote(pool.at[d, pl.ds(2, 2)], core_part.at[d], core_sem, d, (s, t_core))
 
     def x_copy(d):
-        return remote(x_stage.at[d], x_part.at[d], x_sem, d, (s, t_x))
+        return remote(pool.at[d, 1], x_part.at[d], x_sem, d, (s, t_x))
 
     def ret_copy(d):
         return remote(
-            back_stage.at[d], back.at[d], ret_sem, d, (lax.rem(s - d + n_sp, n_sp), t)
+            pool.at[d, 0], back.at[d], ret_sem, d, (partner(s, d), t)
         )
 
     for load in loads[1:]:
@@ -285,20 +286,20 @@
         up_act = jnp.dot(picked, wu[...], preferred_element_type=F32)
         hidden = (gate_act / (1.0 + jnp.exp(-gate_act)) * up_act).astype(BF16)
         part = jnp.dot(hidden, wd[...], preferred_element_type=F32)
-        pool[d, pl.ds(2, 2)] = part[2 * capp :].astype(BF16).reshape(2, capp, width)
-        kept[lax.rem(d, 2)] = part[: 2 * capp]
+        for copy in (xf_copy, cf_copy, cf2_copy):
+            copy(d).wait_send()
+        pool[d] = part.astype(BF16).reshape(4, capp, width)
         core_copy(d).start()
 
     def over_cores(d):
         core_copy(d).wait_recv()
-        both = kept[lax.rem(d, 2)] + core_part[d].reshape(2 * capp, width).astype(F32)
-        x_stage[d] = both[capp:].astype(BF16)
-        kept_own[lax.rem(d, 2)] = both[:capp]
+        both = pool[d, pl.ds(0, 2)].astype(F32) + core_part[d].astype(F32)
+        pool[d, pl.ds(0, 2)] = both.astype(BF16)
         x_copy(d).start()
 
     def over_x(d):
         x_copy(d).wait_recv()
-        done = (kept_own[lax.rem(d, 2)] + x_part[d].astype(F32)).astype(BF16)
+        done = (pool[d, 0].astype(F32) + x_part[d].astype(F32)).astype(BF16)
 
         @pl.when(d == 0)
         def _():
@@ -306,22 +307,26 @@
 
         @pl.when(d > 0)
         def _():
-            back_stage[d] = done
+            pool[d, 0] = done
             ret_copy(d).start()
 
-    def pipeline(i):
+    def inward(i):
         stage(i, 0, arrive)
         stage(i, 1, relay)
-        stage(i, 4, over_x)
-        stage(i, 3, over_cores)
         stage(i, 2, compute)
 
-    each(0, n_sp + 4, pipeline)
+    each(0, n_sp + 2, inward)
+
+    def outward(i):
+        stage(i, 0, lambda d: over_cores(n_sp - 1 - d))
+        stage(i, 2, lambda d: over_x(n_sp - 1 - d))
+
+    each(0, n_sp + 2, outward)
 
     combine = jnp.zeros((tok_row, slots), F32)
     for k in range(top):
         combine = combine + jnp.where(
-            slot_of_col == slot_col[k], route_weight_ref[:, k : k + 1], 0.0
+            slot_of_col == slot_col[k], upright(route_weight_ref[k : k + 1, :]), 0.0
         )
     high = combine.astype(BF16)
     low = (combine - high.astype(F32)).astype(BF16)
@@ -333,8 +338,8 @@
     out_ref[...] = (stream[...] + mixture).astype(out_ref.dtype)
 
     def sent_kv(d):
-        kv_copy(d).wait_send()
-        gate_copy(d).wait_send()
+        for copy in kv_copies(d):
+            copy.wait_send()
 
     each(1, n_sp - s, sent_kv)
     for k in range(1, n_tp):
@@ -346,7 +351,7 @@
             disp_copy(d).wait_send()
             ret_copy(d).wait_send()
 
-        for copy in (xf_copy, cf_copy, cf2_copy, core_copy, x_copy):
+        for copy in (core_copy, x_copy):
             copy(d).wait_send()
 
     each(0, n_sp, sent)
@@ -370,12 +375,11 @@
 ):
     tok = queries.shape[0]
     heads = forget_prefix_log.shape[1]
-    assert keys.shape[1] == HEAD_DIM and n_tp == 4
+    assert keys.shape[1] == HEAD_DIM and n_tp == 4 and n_sp & (n_sp - 1) == 0
     tok_row, width = residual.shape
     capacity = max(2, 2 * tok_row * routes.shape[1] // n_sp)
     capp = -(-capacity // 16) * 16
     quarter = w_gate.shape[2]
-    kv = jnp.concatenate([keys, values], axis=1)
     vmem = pl.BlockSpec(memory_space=pltpu.VMEM)
     hbm = pl.BlockSpec(memory_space=pl.ANY)
     sems = lambda n: pltpu.SemaphoreType.DMA((2, n))
@@ -386,7 +390,7 @@
         in_specs=[vmem] * 8 + [hbm] * 4,
         out_specs=vmem,
         scratch_shapes=[
-            pltpu.VMEM((n_sp, tok, 2 * HEAD_DIM), BF16),
+            pltpu.VMEM((n_sp, 2 * HEAD_DIM, tok), BF16),
             pltpu.VMEM((n_sp, heads, tok), F32),
             pltpu.VMEM((tok, heads * HEAD_DIM), BF16),
             pltpu.VMEM((n_tp, tok_row, heads * HEAD_DIM), BF16),
@@ -400,11 +404,8 @@
             pltpu.VMEM((n_sp, 2, capp, width), BF16),
             pltpu.VMEM(block, BF16),
             pltpu.VMEM(block, BF16),
-            pltpu.VMEM(block, BF16),
-            pltpu.VMEM(block, BF16),
-            pltpu.VMEM((2, 2 * capp, width), F32),
-            pltpu.VMEM((2, capp, width), F32),
             pltpu.SemaphoreType.DMA((4,)),
+            sems(n_sp),
             sems(n_sp),
             sems(n_sp),
             sems(n_tp),
@@ -421,13 +422,13 @@
         ),
     )(
         queries,
-        kv,
+        keys.T,
+        values.T,
         forget_prefix_log.T,
         residual,
         norm_gain.reshape(1, width),
-        routes,
         routes.T,
-        route_weight,
+        route_weight.T,
         out_weight,
         w_gate,
         w_up,

time: 72.5 us -> 62.2 us (0.86)
  Pallas kernels: 65.4 us -> 60.4 us
  local copies, waits for them, and re-layouts: 5.93 us -> 1.57 us
    pallas_call x1, Pallas kernels: 65.4 us -> 60.4 us  [shards(): pl.pallas_call(functools.partial(layer_kernel, n_sp, n_tp), out_shape=jax...]
    unnamed x5 -> x1, local copies, waits for them, and re-layouts: 5.93 us -> 1.57 us
where the time goes in v2:
time: 62.2 us; the launch traced here: 62 us
  Pallas kernels  60.4 us (97%)
  local copies, waits for them, and re-layouts  1.57 us (3%)
    pallas_call x1, Pallas kernels, shards(): pl.pallas_call(functools.partial(layer_kernel, n_sp, n_tp), out_shape=jax...  60.4 us
    unnamed x1, local copies, waits for them, and re-layouts  1.57 us

profile of v2, /device:TPU:0, one launch (start us, length us, event | category | flops | bytes accessed | tf_op | source)
XLA Modules:
  0.0 62.0 jit_solution(1986260294655186880)
XLA Ops:
  0.0 60.4 %shard_map.118 = bf16[32,2048]{1,0:T(8,128)(2,1)} custom-call(bf16[128,256]{1,0:T(8,128)(2,1)} %q_ref.1, bf16[64,128]{1,0:T(8,128)(2,1)} %bitcast.6, bf16[64,128]{1,0:T(8,128)(2,1)} %bitcast.7, f32[4,128]{1,0:T(4,128)} %bitcast.9, bf16[32,2048]{1,0:T(8,128)(2,1)} %residual_ref.1, f32[1,2048]{1,0:T(1,128)} %bitcast.8, s32[2,32]{1,0:T(2,128)} %bitcast.10, ...), custom_call_target="tpu_custom_call" | custom-call | tf_op jit(solution)/shard_map/pallas_call | solution.py:387
  60.4 1.6 %copy.14 = bf16[32,2048]{1,0:T(8,128)(2,1)} copy(bf16[32,2048]{1,0:T(8,128)(2,1)} %shard_map.118) | data formatting | bytes 262144
